TPU v7x, 32 devices: a whole 2x2x4 slice. The times are simulated.
32 devices in a mesh: fs: 16 (over z, y, x), tp: 2 (over core).
Axes of the slice: x: 2, y: 2, z: 4, core: 2. Of those that a mesh axis runs over, the one named last changes fastest.
Arguments:
- tokens: bfloat16 [6144, 2048], P('fs', 'tp'), may hold values from -8 to 8
- w_value: bfloat16 [2048, 1024], P('fs', 'tp'), may hold values from -0.125 to 0.125
- w_gate: bfloat16 [2048, 1024], P('fs', 'tp'), may hold values from -0.125 to 0.125
- conv_kernel: bfloat16 [31, 1024], replicated, may hold values from -1 to 1
- conv_gain: float32 [1024], replicated, may hold values from 0.1 to 1.9
- w_mix_out: bfloat16 [1024, 2048], P('fs', 'tp'), may hold values from -0.1875 to 0.1875
- mix_gain: float32 [2048], replicated, may hold values from 0.1 to 1.9
- w_up: bfloat16 [2048, 8192], P('fs', 'tp'), may hold values from -0.125 to 0.125
- w_down: bfloat16 [8192, 2048], P('tp', 'fs'), may hold values from -0.0625 to 0.0625
- out_gain: float32 [2048], replicated, may hold values from 0.1 to 1.9
Outputs:
- result: bfloat16 [6144, 2048], P('fs', 'tp')
All inputs are finite; a program needn't handle non-finite values.
Results may differ from a plain program's by a relative error of at most 0.013.
Values may be sent and summed in bfloat16 or wider, within the bound.
A program may use at most 128 MiB of HBM per device.

v0:
```python
import jax
import jax.numpy as jnp
from jax import lax
from jax.sharding import PartitionSpec as P

WIDTH = 2048
CHANNELS = 1024
KERNEL = 31
LENGTH = 128
norm_eps = 1e-05
residual_scale = 2.0**0.5


def causal_filter(gated, kernel):
    sequences = gated.shape[0] // LENGTH
    frames = gated.astype(jnp.float32).reshape(sequences, LENGTH, gated.shape[1])
    padded = jnp.pad(frames, ((0, 0), (KERNEL - 1, 0), (0, 0)))
    accumulated = jnp.zeros(frames.shape, jnp.float32)
    for offset in range(KERNEL):
        accumulated = (
            accumulated + kernel[offset].astype(jnp.float32) * padded[:, offset : offset + LENGTH]
        )
    return accumulated.reshape(gated.shape[0], gated.shape[1])


def normalize(values, total_sum, total_sq, entries, gain_vector):
    average = total_sum / entries
    spread = jnp.maximum(total_sq / entries - average * average, 0.0)
    return (values - average[:, None]) * lax.rsqrt(spread[:, None] + norm_eps) * gain_vector


def add_rows(piece, source):
    return jnp.dot(source, piece, preferred_element_type=jnp.float32)


def add_pair(pieces, source):
    first = jnp.dot(source, pieces[0], preferred_element_type=jnp.float32)
    second = jnp.dot(source, pieces[1], preferred_element_type=jnp.float32)
    return (first, second)


def per_device(
    tokens, w_value, w_gate, conv_kernel, conv_gain, w_mix_out, mix_gain, w_up, w_down, out_gain
):
    tp_rank = lax.axis_index("tp")
    width_part = tokens.shape[1]
    channel_part = w_value.shape[1]
    features = lax.all_gather(tokens, "tp", axis=1, tiled=True)
    values_proj, gate_proj = add_pair(
        (
            lax.all_gather(w_value, "fs", axis=0, tiled=True),
            lax.all_gather(w_gate, "fs", axis=0, tiled=True),
        ),
        source=features,
    )
    gated = (values_proj * jax.nn.sigmoid(gate_proj)).astype(jnp.bfloat16)
    kernel = lax.dynamic_slice_in_dim(conv_kernel, tp_rank * channel_part, channel_part, 1)
    filtered = causal_filter(gated, kernel)
    channel_sum, channel_sq = lax.psum(
        (jnp.sum(filtered, 1), jnp.sum(filtered * filtered, 1)), "tp"
    )
    channel_gain = lax.dynamic_slice_in_dim(conv_gain, tp_rank * channel_part, channel_part, 0)
    activated = jax.nn.silu(
        normalize(filtered, channel_sum, channel_sq, CHANNELS, channel_gain)
    ).astype(jnp.bfloat16)
    all_channels = lax.all_gather(activated, "tp", axis=1, tiled=True)
    mixed = add_rows(lax.all_gather(w_mix_out, "fs", axis=0, tiled=True), source=all_channels)
    combined = residual_scale * tokens.astype(jnp.float32) + mixed
    middle_sum, middle_sq = lax.psum((jnp.sum(combined, 1), jnp.sum(combined * combined, 1)), "tp")
    middle_gain = lax.dynamic_slice_in_dim(mix_gain, tp_rank * width_part, width_part, 0)
    middle = normalize(combined, middle_sum, middle_sq, WIDTH, middle_gain).astype(jnp.bfloat16)
    middle_whole = lax.all_gather(middle, "tp", axis=1, tiled=True)
    up_proj = add_rows(lax.all_gather(w_up, "fs", axis=0, tiled=True), source=middle_whole)
    hidden = jnp.square(jax.nn.relu(up_proj)).astype(jnp.bfloat16)
    terms = jnp.dot(
        hidden, lax.all_gather(w_down, "fs", axis=1, tiled=True), preferred_element_type=jnp.float32
    )
    down_sum = lax.psum_scatter(
        terms.astype(jnp.bfloat16), "tp", scatter_dimension=1, tiled=True
    ).astype(jnp.float32)
    final = residual_scale * middle.astype(jnp.float32) + down_sum
    final_sum, final_sq = lax.psum((jnp.sum(final, 1), jnp.sum(final * final, 1)), "tp")
    final_gain = lax.dynamic_slice_in_dim(out_gain, tp_rank * width_part, width_part, 0)
    return normalize(final, final_sum, final_sq, WIDTH, final_gain).astype(jnp.bfloat16)


def solution(mesh):
    in_specs = (
        P("fs", "tp"),
        P("fs", "tp"),
        P("fs", "tp"),
        P(),
        P(),
        P("fs", "tp"),
        P(),
        P("fs", "tp"),
        P("tp", "fs"),
        P(),
    )
    out_specs = P("fs", "tp")
    return jax.shard_map(
        per_device, mesh=mesh, in_specs=in_specs, out_specs=out_specs, check_vma=False
    )
```

profile of v0, /device:TPU:0, one launch (start us, length us, event | category | flops | bytes accessed | tf_op | source)
XLA Modules:
  0.0 715.3 jit_solution(9099667638542839668)
XLA Ops:
  6.5 0.7 all-gather.8.cloned.1.call-update
  7.3 0.7 all-gather.12.cloned.1.call-update
  8.1 0.7 all-gather.10.cloned.1.call-update
  8.8 0.5 all-gather.14.cloned.1.call-update
  9.4 0.8 dynamic_slice.13
  10.1 0.7 dynamic_slice.14
  10.8 1.2 dynamic-slice_convert_fusion.29
  12.0 1.2 dynamic-slice_convert_fusion.30
  13.2 8.2 %all-gather.8.cloned.1.call-done = bf16[384,2048]{1,0:T(8,128)(2,1)} async-done(((bf16[384,1024]{1,0:T(8,128)(2,1)}), bf16[384,2048]{1,0:T(8,128)(2,1)}) %all-gather.8.cloned.1.call-update) | async-done | bytes 1572880 | tf_op jit(solution)/shard_map/all_gather | solution.py:48
  21.4 64.4 %all-gather.12.cloned.1.call-done = bf16[2048,512]{1,0:T(8,128)(2,1)} async-done(((bf16[128,512]{1,0:T(8,128)(2,1)}), bf16[2048,512]{1,0:T(8,128)(2,1)}) %all-gather.12.cloned.1.call-update) | async-done | bytes 2097168 | tf_op jit(solution)/shard_map/all_gather | solution.py:52
  85.8 3.2 fusion.5
  88.9 58.8 %all-gather.10.cloned.1.call-done = bf16[2048,512]{1,0:T(8,128)(2,1)} async-done(((bf16[128,512]{1,0:T(8,128)(2,1)}), bf16[2048,512]{1,0:T(8,128)(2,1)}) %all-gather.10.cloned.1.call-update) | async-done | bytes 2097168 | tf_op jit(solution)/shard_map/all_gather | solution.py:51
  147.8 2.6 fusion.6
  150.4 3.5 fusion.72
  154.0 2.6 all-reduce.3
  156.6 0.3 multiply_convert_fusion.3
  156.9 2.4 all_gather.27
  159.3 50.3 %all-gather.14.cloned.1.call-done = bf16[1024,1024]{1,0:T(8,128)(2,1)} async-done(((bf16[64,1024]{1,0:T(8,128)(2,1)}), bf16[1024,1024]{1,0:T(8,128)(2,1)}) %all-gather.14.cloned.1.call-update) | async-done | bytes 2097168 | tf_op jit(solution)/shard_map/all_gather | solution.py:67
  209.6 2.8 fusion.71
  212.4 2.5 all-reduce.2
  214.9 1.2 multiply_convert_fusion.2
  216.1 0.5 all-gather.18.cloned.1.call-update
  216.7 0.7 all-gather.20.cloned.1.call-update
  217.4 0.2 reduce-scatter.2.cloned.1.call-start
  217.6 7.2 %all-gather.16.cloned.1.call-done = bf16[384,2048]{1,0:T(8,128)(2,1)} async-done(((bf16[384,1024]{1,0:T(8,128)(2,1)}), bf16[384,2048]{1,0:T(8,128)(2,1)}) %all-gather.16.cloned.1.call-update) | async-done | bytes 1572880 | tf_op jit(solution)/shard_map/all_gather | solution.py:72
  224.8 194.8 %all-gather.18.cloned.1.call-done = bf16[2048,4096]{1,0:T(8,128)(2,1)} async-done(((bf16[128,4096]{1,0:T(8,128)(2,1)}), bf16[2048,4096]{1,0:T(8,128)(2,1)}) %all-gather.18.cloned.1.call-update) | async-done | bytes 16777232 | tf_op jit(solution)/shard_map/all_gather | solution.py:73
  419.6 250.0 %all-gather.20.cloned.1.call-done = bf16[4096,2048]{1,0:T(8,128)(2,1)} async-done(((bf16[4096,128]{1,0:T(8,128)(2,1)}), bf16[4096,2048]{1,0:T(8,128)(2,1)}) %all-gather.20.cloned.1.call-update) | async-done | bytes 16777232 | tf_op jit(solution)/shard_map/all_gather | solution.py:76
  669.6 25.3 %fusion.2 = bf16[384,2048]{1,0:T(8,128)(2,1)} fusion(bf16[4096,2048]{1,0:T(8,128)(2,1)} %all-gather.20.cloned.1.call-done, bf16[384,2048]{1,0:T(8,128)(2,1)} %all-gather.16.cloned.1.call-done, bf16[2048,4096]{1,0:T(8,128)(2,1)} %all-gather.18.cloned.1.call-done), kind=kOutput, calls=%fused_computation.3 | convolution fusion | flops 12890406912 | bytes 36700160 | tf_op jit(solution)/shard_map/dot_general | solution.py:75
  695.0 7.3 %reduce-scatter.2.cloned.1.call-done = bf16[384,1024]{1,0:T(8,128)(2,1)} async-done(((bf16[384,2048]{1,0:T(8,128)(2,1)}), bf16[384,1024]{1,0:T(8,128)(2,1)}) %reduce-scatter.2.cloned.1.call-update) | async-done | bytes 786448 | tf_op jit(solution)/shard_map/reduce_scatter | solution.py:78
  702.2 1.9 fusion.7
  704.1 2.5 all-reduce.1
  706.6 1.9 multiply_convert_fusion.1
  (21 shorter events, 0.4 us)
Async XLA Ops:
  6.5 14.9 %all-gather.8.cloned.1.call-start = ((), (), s32[]{:S(2)}) async-start(), calls=%async_computation.1 | async-start | bytes 2359296 | tf_op jit(solution)/shard_map/all_gather | solution.py:48
  7.3 78.5 %all-gather.12.cloned.1.call-start = ((), (), s32[]{:S(2)}) async-start(), calls=%async_computation.3 | async-start | bytes 2228224 | tf_op jit(solution)/shard_map/all_gather | solution.py:52
  8.0 139.8 %all-gather.10.cloned.1.call-start = ((), (), s32[]{:S(2)}) async-start(), calls=%async_computation.2 | async-start | bytes 2228224 | tf_op jit(solution)/shard_map/all_gather | solution.py:51
  8.7 200.9 %all-gather.14.cloned.1.call-start = ((), (), s32[]{:S(2)}) async-start(), calls=%async_computation.4 | async-start | bytes 2228224 | tf_op jit(solution)/shard_map/all_gather | solution.py:67
  9.3 215.5 %all-gather.16.cloned.1.call-start = ((), (), s32[]{:S(2)}) async-start(), calls=%async_computation.5 | async-start | bytes 2359296 | tf_op jit(solution)/shard_map/all_gather | solution.py:72
  21.4 126.3 %copy-start.2 = (bf16[384,2048]{1,0:T(8,128)(2,1)S(1)}, bf16[384,2048]{1,0:T(8,128)(2,1)}, u32[]{:S(2)}) copy-start(bf16[384,2048]{1,0:T(8,128)(2,1)} %all-gather.8.cloned.1.call-done) | copy-start | bytes 4718596
  154.0 55.6 %copy-start.1 = (bf16[384,1024]{1,0:T(8,128)(2,1)S(1)}, bf16[384,1024]{1,0:T(8,128)(2,1)}, u32[]{:S(2)}) copy-start(bf16[384,1024]{1,0:T(8,128)(2,1)} %param.10) | copy-start | bytes 2359300
  216.0 203.6 %all-gather.18.cloned.1.call-start = ((), (), s32[]{:S(2)}) async-start(), calls=%async_computation.6 | async-start | bytes 17825792 | tf_op jit(solution)/shard_map/all_gather | solution.py:73
  216.6 453.0 %all-gather.20.cloned.1.call-start = ((), (), s32[]{:S(2)}) async-start(), calls=%async_computation.7 | async-start | bytes 17825792 | tf_op jit(solution)/shard_map/all_gather | solution.py:76
  217.4 484.9 %reduce-scatter.2.cloned.1.call-start = ((), (), s32[]{:S(2)}) async-start(), calls=%async_computation.8 | async-start | bytes 2359296 | tf_op jit(solution)/shard_map/reduce_scatter | solution.py:78
  694.9 11.6 %dynamic-slice-start = ((f32[2048]{0:T(1024)}, s32[]{:T(128)}), f32[1024]{0:T(1024)S(1)}, s32[]{:S(2)}) async-start(f32[2048]{0:T(1024)} %param.19, s32[]{:T(128)} %select_n.9), calls=%async_computation.9 | async-start | bytes 8704 | tf_op jit(solution)/shard_map/dynamic_slice | solution.py:83
  702.2 4.3 copy-start
Sparse Core Ops, SparseCore 0:
  8.9 12.5 all-gather.7
  24.2 61.5 all-gather.11
  88.6 59.1 all-gather.9
  150.4 59.1 all-gather.13
  216.2 8.5 all-gather.15
  227.4 192.1 all-gather.17
  422.3 247.2 all-gather.19
  695.1 7.1 reduce-scatter.1
where the time goes:
time: 716 us; the launch traced here: 715 us
  waiting for transfers between devices  645 us (90%)
  matrix products  33.7 us (5%)
  between operations  13.6 us (2%)
  other arithmetic  11.3 us (2%)
  blocking collectives  9.91 us (1%)
    all_gather x1, waiting for transfers between devices, per_device(): lax.all_gather(w_down, 'fs', axis=1, tiled=True)  250 us
    all_gather x1, waiting for transfers between devices, per_device(): lax.all_gather(w_up, 'fs', axis=0, tiled=True)  195 us
    all_gather x1, waiting for transfers between devices, per_device(): lax.all_gather(w_gate, 'fs', axis=0, tiled=True)  64.4 us
    all_gather x1, waiting for transfers between devices, per_device(): lax.all_gather(w_value, 'fs', axis=0, tiled=True)  58.8 us
    all_gather x1, waiting for transfers between devices, per_device(): lax.all_gather(w_mix_out, 'fs', axis=0, tiled=True)  50.3 us
    dot_general x1, matrix products, per_device(): jnp.dot(hidden, lax.all_gather(w_down, 'fs', axis=1, tiled=True), preferr...  25.3 us
  transfers between devices with their start and end apart: 8, of which 8 were waited for; matrix products, arithmetic and copies ran while one was open for 2% of the time, Pallas kernels for 0%

commit v1 on v0

--- a/solution.py
+++ b/solution.py
@@ -9,6 +9,12 @@
 LENGTH = 128
 norm_eps = 1e-05
 residual_scale = 2.0**0.5
+
+
+def stack_and_merge(x, mesh_axis, along):
+    parts = lax.all_gather(x, mesh_axis, axis=0, tiled=False)
+    whole = jnp.concatenate(parts, axis=along)
+    return whole
 
 
 def causal_filter(gated, kernel):
@@ -72,9 +78,7 @@
     middle_whole = lax.all_gather(middle, "tp", axis=1, tiled=True)
     up_proj = add_rows(lax.all_gather(w_up, "fs", axis=0, tiled=True), source=middle_whole)
     hidden = jnp.square(jax.nn.relu(up_proj)).astype(jnp.bfloat16)
-    terms = jnp.dot(
-        hidden, lax.all_gather(w_down, "fs", axis=1, tiled=True), preferred_element_type=jnp.float32
-    )
+    terms = jnp.dot(hidden, stack_and_merge(w_down, "fs", 1), preferred_element_type=jnp.float32)
     down_sum = lax.psum_scatter(
         terms.astype(jnp.bfloat16), "tp", scatter_dimension=1, tiled=True
     ).astype(jnp.float32)

time: 716 us -> 647 us (0.904)
  waiting for transfers between devices: 645 us -> 564 us
  local copies, waits for them, and re-layouts: 1.48 us -> 21.7 us
    all_gather x1, waiting for transfers between devices: 250 us -> 185 us  [stack_and_merge(): parts = lax.all_gather(x, mesh_axis, axis=0, tiled=False)]
    reshape x0 -> x1, local copies, waits for them, and re-layouts: none -> 21.6 us  [stack_and_merge(): whole = jnp.concatenate(parts, axis=along)]
    all_gather x1, waiting for transfers between devices: 195 us -> 183 us  [per_device(): lax.all_gather(w_up, 'fs', axis=0, tiled=True)]
    all_gather x1, waiting for transfers between devices: 7.2 us -> 0.01 us  [per_device(): middle_whole = lax.all_gather(middle, 'tp', axis=1, tiled=True)]
  transfers between devices with their start and end apart: 8 -> 8, of which waited for: 8 -> 7; matrix products, arithmetic and copies ran while one was open for 2% -> 6% of each run, Pallas kernels for 0% -> 0%
where the time goes in v1:
time: 647 us; the launch traced here: 646 us
  waiting for transfers between devices  564 us (87%)
  matrix products  27.5 us (4%)
  local copies, waits for them, and re-layouts  21.7 us (3%)
  between operations  13.6 us (2%)
  blocking collectives  9.91 us (2%)
  other arithmetic  9.18 us (1%)
    all_gather x1, waiting for transfers between devices, stack_and_merge(): parts = lax.all_gather(x, mesh_axis, axis=0, tiled=False)  185 us
    all_gather x1, waiting for transfers between devices, per_device(): lax.all_gather(w_up, 'fs', axis=0, tiled=True)  183 us
    all_gather x1, waiting for transfers between devices, per_device(): lax.all_gather(w_gate, 'fs', axis=0, tiled=True)  64.4 us
    all_gather x1, waiting for transfers between devices, per_device(): lax.all_gather(w_value, 'fs', axis=0, tiled=True)  58.8 us
    all_gather x1, waiting for transfers between devices, per_device(): lax.all_gather(w_mix_out, 'fs', axis=0, tiled=True)  50.3 us
    reshape x1, local copies, waits for them, and re-layouts, stack_and_merge(): whole = jnp.concatenate(parts, axis=along)  21.6 us
    dot_general x1, matrix products, per_device(): jnp.dot(hidden, stack_and_merge(w_down, 'fs', 1), preferred_element_type=...  19 us
  transfers between devices with their start and end apart: 8, of which 7 were waited for; matrix products, arithmetic and copies ran while one was open for 6% of the time, Pallas kernels for 0%

profile of v1, /device:TPU:0, one launch (start us, length us, event | category | flops | bytes accessed | tf_op | source)
XLA Modules:
  0.0 645.9 jit_solution(10999383407543221845)
XLA Ops:
  6.5 0.7 all-gather.9.cloned.1.call-update
  7.3 0.7 all-gather.13.cloned.1.call-update
  8.1 0.7 all-gather.11.cloned.1.call-update
  8.8 0.5 all-gather.15.cloned.1.call-update
  9.4 0.5 all-gather.21.cloned.1.call-update
  10.0 0.1 dynamic_slice.13
  10.1 0.1 dynamic-slice_convert_fusion.29
  10.2 0.2 dynamic-slice_convert_fusion.30
  10.4 11.1 %all-gather.9.cloned.1.call-done = bf16[384,2048]{1,0:T(8,128)(2,1)} async-done(((bf16[384,1024]{1,0:T(8,128)(2,1)}), bf16[384,2048]{1,0:T(8,128)(2,1)}) %all-gather.9.cloned.1.call-update) | async-done | bytes 1572880 | tf_op jit(solution)/shard_map/all_gather | solution.py:54
  21.4 64.4 %all-gather.13.cloned.1.call-done = bf16[2048,512]{1,0:T(8,128)(2,1)} async-done(((bf16[128,512]{1,0:T(8,128)(2,1)}), bf16[2048,512]{1,0:T(8,128)(2,1)}) %all-gather.13.cloned.1.call-update) | async-done | bytes 2097168 | tf_op jit(solution)/shard_map/all_gather | solution.py:58
  85.8 3.2 fusion.4
  89.0 58.8 %all-gather.11.cloned.1.call-done = bf16[2048,512]{1,0:T(8,128)(2,1)} async-done(((bf16[128,512]{1,0:T(8,128)(2,1)}), bf16[2048,512]{1,0:T(8,128)(2,1)}) %all-gather.11.cloned.1.call-update) | async-done | bytes 2097168 | tf_op jit(solution)/shard_map/all_gather | solution.py:57
  147.8 2.6 fusion.5
  150.3 0.1 convert.32
  150.4 3.5 fusion.71
  154.0 2.6 all-reduce.3
  156.6 0.3 multiply_convert_fusion.3
  156.9 2.4 all_gather.30
  159.3 50.3 %all-gather.15.cloned.1.call-done = bf16[1024,1024]{1,0:T(8,128)(2,1)} async-done(((bf16[64,1024]{1,0:T(8,128)(2,1)}), bf16[1024,1024]{1,0:T(8,128)(2,1)}) %all-gather.15.cloned.1.call-update) | async-done | bytes 2097168 | tf_op jit(solution)/shard_map/all_gather | solution.py:73
  209.6 2.8 fusion.70
  212.4 2.5 all-reduce.2
  214.9 1.2 multiply_convert_fusion.2
  216.0 0.0 all-gather.19.cloned.1.call-start
  216.1 0.7 all-gather.19.cloned.1.call-update
  216.8 185.2 %all-gather.21.cloned.1.call-done = bf16[65536,128]{1,0:T(8,128)(2,1)} async-done(((bf16[4096,128]{1,0:T(8,128)(2,1)}), bf16[65536,128]{1,0:T(8,128)(2,1)}) %all-gather.21.cloned.1.call-update) | async-done | bytes 16777232 | tf_op jit(solution)/shard_map/all_gather | solution.py:15
  402.1 21.6 %copy.11 = bf16[4096,16,128]{0,2,1:T(8,128)(2,1)} copy(bf16[4096,16,128]{2,0,1:T(8,128)(2,1)} %bitcast.56) | data formatting | bytes 33554432 | tf_op jit(solution)/shard_map/reshape | solution.py:16
  423.6 182.8 %all-gather.19.cloned.1.call-done = bf16[2048,4096]{1,0:T(8,128)(2,1)} async-done(((bf16[128,4096]{1,0:T(8,128)(2,1)}), bf16[2048,4096]{1,0:T(8,128)(2,1)}) %all-gather.19.cloned.1.call-update) | async-done | bytes 16777232 | tf_op jit(solution)/shard_map/all_gather | solution.py:79
  606.5 19.0 %fusion.1 = bf16[384,2048]{1,0:T(8,128)(2,1)} fusion(bf16[4096,2048]{0,1:T(8,128)(2,1)} %bitcast.57, bf16[384,2048]{1,0:T(8,128)(2,1)} %all-gather.17.cloned.1.call-done, bf16[2048,4096]{1,0:T(8,128)(2,1)} %all-gather.19.cloned.1.call-done), kind=kOutput, calls=%fused_computation.2 | convolution fusion | flops 12890406912 | bytes 36700160 | tf_op jit(solution)/shard_map/dot_general | solution.py:81
  625.5 7.3 %reduce-scatter.2.cloned.1.call-done = bf16[384,1024]{1,0:T(8,128)(2,1)} async-done(((bf16[384,2048]{1,0:T(8,128)(2,1)}), bf16[384,1024]{1,0:T(8,128)(2,1)}) %reduce-scatter.2.cloned.1.call-update) | async-done | bytes 786448 | tf_op jit(solution)/shard_map/reduce_scatter | solution.py:82
  632.8 1.9 fusion.6
  634.7 2.5 all-reduce.1
  637.1 1.9 multiply_convert_fusion.1
  (28 shorter events, 0.3 us)
Async XLA Ops:
  6.5 3.4 copy-start.4
  6.5 3.5 copy-start.3
  6.5 3.5 copy-start.2
  6.5 14.9 %all-gather.9.cloned.1.call-start = ((), (), s32[]{:S(2)}) async-start(), calls=%async_computation.1 | async-start | bytes 2359296 | tf_op jit(solution)/shard_map/all_gather | solution.py:54
  7.3 78.5 %all-gather.13.cloned.1.call-start = ((), (), s32[]{:S(2)}) async-start(), calls=%async_computation.3 | async-start | bytes 2228224 | tf_op jit(solution)/shard_map/all_gather | solution.py:58
  8.0 139.8 %all-gather.11.cloned.1.call-start = ((), (), s32[]{:S(2)}) async-start(), calls=%async_computation.2 | async-start | bytes 2228224 | tf_op jit(solution)/shard_map/all_gather | solution.py:57
  8.7 200.9 %all-gather.15.cloned.1.call-start = ((), (), s32[]{:S(2)}) async-start(), calls=%async_computation.4 | async-start | bytes 2228224 | tf_op jit(solution)/shard_map/all_gather | solution.py:73
  9.3 392.7 %all-gather.21.cloned.1.call-start = ((), (), s32[]{:S(2)}) async-start(), calls=%async_computation.8 | async-start | bytes 17825792 | tf_op jit(solution)/shard_map/all_gather | solution.py:15
  9.9 413.7 %all-gather.17.cloned.1.call-start = ((), (), s32[]{:S(2)}) async-start(), calls=%async_computation.5 | async-start | bytes 2359296 | tf_op jit(solution)/shard_map/all_gather | solution.py:78
  21.4 126.3 %copy-start.5 = (bf16[384,2048]{1,0:T(8,128)(2,1)S(1)}, bf16[384,2048]{1,0:T(8,128)(2,1)}, u32[]{:S(2)}) copy-start(bf16[384,2048]{1,0:T(8,128)(2,1)} %all-gather.9.cloned.1.call-done) | copy-start | bytes 4718596
  154.0 55.6 %copy-start.1 = (bf16[384,1024]{1,0:T(8,128)(2,1)S(1)}, bf16[384,1024]{1,0:T(8,128)(2,1)}, u32[]{:S(2)}) copy-start(bf16[384,1024]{1,0:T(8,128)(2,1)} %param.10) | copy-start | bytes 2359300
  216.0 390.4 %all-gather.19.cloned.1.call-start = ((), (), s32[]{:S(2)}) async-start(), calls=%async_computation.6 | async-start | bytes 17825792 | tf_op jit(solution)/shard_map/all_gather | solution.py:79
  216.8 416.0 %reduce-scatter.2.cloned.1.call-start = ((), (), s32[]{:S(2)}) async-start(), calls=%async_computation.7 | async-start | bytes 2359296 | tf_op jit(solution)/shard_map/reduce_scatter | solution.py:82
  625.5 11.6 %dynamic-slice-start = ((f32[2048]{0:T(1024)}, s32[]{:T(128)}), f32[1024]{0:T(1024)S(1)}, s32[]{:S(2)}) async-start(f32[2048]{0:T(1024)} %param.19, s32[]{:T(128)} %select_n.9), calls=%async_computation.9 | async-start | bytes 8704 | tf_op jit(solution)/shard_map/dynamic_slice | solution.py:87
  632.8 4.3 copy-start
Sparse Core Ops, SparseCore 0:
  8.9 12.5 all-gather.8
  24.2 61.5 all-gather.12
  88.6 59.1 all-gather.10
  150.4 59.1 all-gather.14
  212.2 189.7 all-gather.20
  403.5 7.9 all-gather.16
  414.2 192.1 all-gather.18
  625.6 7.1 reduce-scatter.1
